TPU v7x, 256 devices: a whole 4x4x8 slice. The times are simulated.
256 devices in a mesh: sp: 64 (over z, x, core), tp: 4 (over y).
Axes of the slice: x: 4, y: 4, z: 8, core: 2. Of those that a mesh axis runs over, the one named last changes fastest.
Arguments:
- conv_in: bfloat16 [49152, 1024], P('sp', 'tp'), may hold values from -6 to 6
- conv_pre: bfloat16 [49152, 1024], P('sp', 'tp'), may hold values from -6 to 6
- conv_post: bfloat16 [49152, 1024], P('sp', 'tp'), may hold values from -6 to 6
- taps: float32 [3, 1024], P(None, 'tp'), may hold values from -3 to 3
- out_proj: bfloat16 [1024, 2048], P('tp'), may hold values from -0.1875 to 0.1875
- stream: bfloat16 [49152, 2048], P(('sp', 'tp')), may hold values from -6 to 6
- norm_gain: float32 [2048], replicated, may hold values from 0.1 to 1.9
- routes: int32 [49152, 2], P(('sp', 'tp')), may hold values from 0 to 63, all different within a row; in each aligned block of 192 rows (0 to 191, 192 to 383, ...) at most 8 rows name the same one
- route_weight: float32 [49152, 2], P(('sp', 'tp')), may hold values from 0.1 to 1
- gate_w: bfloat16 [64, 2048, 2048], P('sp', None, 'tp'), may hold values from -0.52734375 to 0.52734375
- up_w: bfloat16 [64, 2048, 2048], P('sp', None, 'tp'), may hold values from -0.52734375 to 0.52734375
- down_w: bfloat16 [64, 2048, 2048], P('sp', 'tp'), may hold values from -0.013244629 to 0.013244629
Outputs:
- output: bfloat16 [49152, 2048], P(('sp', 'tp'))
Inputs may be any that keep to these rules, and one draw needn't show every extreme that they name: `routes`: each row names 2 different experts. In each aligned block of 192 rows no expert is named more than 8 times, a bound that some block reaches.
All inputs are finite; a program needn't handle non-finite values.
Results may differ from a plain program's by a relative error of at most 0.015.
Values may be sent and summed in bfloat16 or wider, within the bound.
A program may use at most 128 MiB of HBM per device.

v0:
```python
import jax
import jax.numpy as jnp
from jax import lax
from jax.sharding import PartitionSpec as P

EPSILON = 1e-05
LIMIT = 7.0
ALPHA = 1.702


def with_halo(x, sides, width):
    for axis, dim in sides:
        count, length = (lax.axis_size(axis), x.shape[dim])
        up = [(i, (i + 1) % count) for i in range(count - 1)]
        down = [(j, i) for i, j in up]
        last = lax.slice_in_dim(x, length - width, length, axis=dim)
        first = lax.slice_in_dim(x, 0, width, axis=dim)
        before = lax.ppermute(last, axis, up)
        after = lax.ppermute(first, axis, down)
        x = jnp.concatenate([before, x, after], axis=dim)
    return x


def cut_along(x, dim, count):
    shape = x.shape
    pieces = x.reshape(*shape[:dim], count, shape[dim] // count, *shape[dim + 1 :])
    return jnp.moveaxis(pieces, dim, 0)


def sent_and_summed(x, axis, dim):
    pieces = cut_along(x, dim, lax.axis_size(axis))
    arrived = lax.all_to_all(pieces, axis, split_axis=0, concat_axis=0, tiled=True)
    return arrived.astype(jnp.float32).sum(axis=0)


def grouped_exchange(x, axis, split_dim, concat_dim, work, item_dim, out_dim):
    items = jax.tree.leaves(x)[0].shape[item_dim]
    count = 2 if items % 2 == 0 else 1
    done = []
    for k in range(count):
        group = jax.tree.map(
            lambda a: lax.slice_in_dim(
                a, k * (items // count), (k + 1) * (items // count), axis=item_dim
            ),
            x,
        )
        done.append(
            work(
                lax.all_to_all(
                    group, axis, split_axis=split_dim, concat_axis=concat_dim, tiled=True
                )
            )
        )
    return jax.tree.map(lambda *parts: jnp.concatenate(parts, axis=out_dim), *done)


def clamped_unit(gate_pre, up_pre):
    gated = jnp.minimum(gate_pre, LIMIT)
    upward = jnp.clip(up_pre, -LIMIT, LIMIT)
    return (upward + 1.0) * gated * jax.nn.sigmoid(ALPHA * gated)


def block_ranks(chosen, block_rows, count):
    shaped = chosen.reshape(-1, block_rows)
    onehot = (shaped[:, :, None] == jnp.arange(count, dtype=jnp.int32)[None, None, :]).astype(
        jnp.int32
    )
    running = jnp.cumsum(onehot, axis=1) - 1
    return jnp.sum(running * onehot, axis=2).reshape(-1)


def local(
    conv_in,
    conv_pre,
    conv_post,
    taps,
    out_proj,
    stream,
    norm_gain,
    routes,
    route_weight,
    gate_w,
    up_w,
    down_w,
):
    product = conv_pre.astype(jnp.float32) * conv_in.astype(jnp.float32)
    padded = with_halo(product.astype(jnp.bfloat16), (("sp", 0),), 1).astype(product.dtype)
    convolved = taps[0] * padded[:-2] + taps[1] * padded[1:-1] + taps[2] * padded[2:]
    mixed = (conv_post.astype(jnp.float32) * convolved).astype(jnp.bfloat16)
    own_rows = stream.shape[0]
    width = stream.shape[1]
    branch = sent_and_summed(
        jnp.dot(mixed, out_proj, preferred_element_type=jnp.float32).astype(jnp.bfloat16), "tp", 0
    )
    resid = (stream.astype(jnp.float32) + branch).astype(jnp.bfloat16)
    resid_f = resid.astype(jnp.float32)
    scale = lax.rsqrt(jnp.mean(resid_f * resid_f, axis=-1, keepdims=True) + EPSILON)
    normed = (resid_f * scale * norm_gain).astype(jnp.bfloat16)
    group_rows, group_routes = (
        lax.all_gather(normed, "tp", axis=0, tiled=True),
        lax.all_gather(routes, "tp", axis=0, tiled=True),
    )
    top_count = routes.shape[1]
    quarters = lax.axis_size("tp")
    experts = gate_w.shape[0] * lax.axis_size("sp")
    capacity = max(2, own_rows * top_count * 4 // (3 * experts))
    group_flat = group_routes.reshape(-1)
    group_rank = block_ranks(group_flat, own_rows * top_count, experts)
    entry_ids = jnp.arange(group_flat.shape[0], dtype=jnp.int32)
    quarter_ids = entry_ids // (own_rows * top_count)
    targets = (group_flat * quarters + quarter_ids) * capacity + group_rank
    outgoing = jnp.zeros((experts * quarters * capacity, width), jnp.bfloat16)
    outgoing = outgoing.at[targets].set(group_rows[entry_ids // top_count])
    outgoing = outgoing.reshape(experts, quarters, capacity, width)

    def expert_work(arrived):
        arrived_shape = arrived.shape
        rows_in = arrived.reshape(-1, width)
        gate_pre = jnp.dot(rows_in, gate_w[0], preferred_element_type=jnp.float32)
        up_pre = jnp.dot(rows_in, up_w[0], preferred_element_type=jnp.float32)
        active = clamped_unit(gate_pre, up_pre).astype(jnp.bfloat16)
        partial_value = jnp.dot(active, down_w[0], preferred_element_type=jnp.float32).reshape(
            arrived_shape
        )
        summed = lax.psum_scatter(
            partial_value.astype(jnp.bfloat16), "tp", scatter_dimension=1, tiled=True
        )
        return lax.all_to_all(summed, "sp", split_axis=0, concat_axis=0, tiled=True)

    returned = grouped_exchange(outgoing, "sp", 0, 0, expert_work, 2, 2)
    back_rows = returned.reshape(-1, width)
    own_flat = routes.reshape(-1)
    own_rank = block_ranks(own_flat, own_rows * top_count, experts)
    picked = back_rows[own_flat * capacity + own_rank].reshape(own_rows, top_count, width)
    total = resid.astype(jnp.float32)
    for column in range(top_count):
        total = total + route_weight[:, column : column + 1] * picked[:, column].astype(jnp.float32)
    return total.astype(jnp.bfloat16)


def solution(mesh):
    placed = (
        P("sp", "tp"),
        P("sp", "tp"),
        P("sp", "tp"),
        P(None, "tp"),
        P("tp", None),
        P(("sp", "tp"), None),
        P(),
        P(("sp", "tp"), None),
        P(("sp", "tp"), None),
        P("sp", None, "tp"),
        P("sp", None, "tp"),
        P("sp", "tp", None),
    )
    return jax.shard_map(
        local, mesh=mesh, in_specs=placed, out_specs=P(("sp", "tp"), None), check_vma=False
    )
```

profile of v0, /device:TPU:1, one launch (start us, length us, event | category | flops | bytes accessed | tf_op | source)
XLA Modules:
  0.0 497.2 jit_solution(11807484701216454249)
XLA Ops:
  7.9 4.5 collective-permute-start
  18.6 40.7 %all_to_all.25 = bf16[4,192,2048]{2,1,0:T(8,128)(2,1)S(1)} all-to-all(bf16[4,192,2048]{2,1,0:T(8,128)(2,1)S(1)} %bitcast.104), channel_id=1, replica_groups=mesh['sp'=64,'tp'=4] {'tp'}, dimensions={0} | all-to-all | bytes 6291456 | tf_op jit(solution)/shard_map/all_to_all | solution.py:32
  62.3 8.1 %all-gather = s32[4,192,2]{1,2,0:T(2,128)S(1)} all-gather(s32[1,192,2]{1,2,0:T(2,128)S(1)} %bitcast.110), channel_id=1, replica_groups=mesh['sp'=64,'tp'=4] {'tp'}, dimensions={0}, use_global_device_ids=true | all-gather | bytes 7680 | tf_op jit(solution)/shard_map/all_gather | solution.py:101
  71.5 6.6 %reduce-window.14 = s32[4,64,3,128]{3,1,2,0:T(8,128)S(1)} reduce-window(s32[4,64,3,128]{3,1,2,0:T(8,128)} %fusion.34, s32[]{:T(128)} %constant.55.clone.1), window={size=1x1x1x128 pad=0_0x0_0x0_0x127_0}, to_apply=%region_1.0 | reduce-window | flops 12484608 | bytes 786436 | tf_op jit(solution)/shard_map/reduce-window
  81.6 24.4 %all-gather.3.cloned.1.call-done = bf16[768,2048]{1,0:T(8,128)(2,1)} async-done(((bf16[192,2048]{1,0:T(8,128)(2,1)}), bf16[768,2048]{1,0:T(8,128)(2,1)}) %all-gather.3.cloned.1.call-update) | async-done | bytes 3145744 | tf_op jit(solution)/shard_map/all_gather | solution.py:100
  106.0 31.9 %scatter_custom_fusion = bf16[2048,2048]{1,0:T(8,128)(2,1)} fusion(s32[1536]{0:T(1024)S(1)} %fusion.40, bf16[768,2048]{1,0:T(8,128)(2,1)} %all-gather.3.cloned.1.call-done, s32[2048]{0:T(1024)S(1)} %pad_clamp_fusion, bf16[]{:T(256)} %constant.28.clone.1), kind=kCustom, calls=%fused_computation.3 | custom fusion | bytes 8389120 | tf_op jit(solution)/shard_map/scatter | solution.py:113
  137.9 11.1 %fusion.47 = (bf16[64,4,4,2048]{3,2,1,0:T(4,128)(2,1)S(1)}, bf16[64,4,4,2048]{3,2,1,0:T(4,128)(2,1)}) fusion(bf16[64,4,8,2048]{3,2,1,0:T(8,128)(2,1)} %bitcast.103), kind=kLoop, calls=%fused_computation.89 | loop fusion | bytes 16777216 | tf_op jit(solution)/shard_map/slice | solution.py:42
  149.0 105.4 %all_to_all.26 = bf16[64,4,4,2048]{3,2,1,0:T(4,128)(2,1)} all-to-all(bf16[64,4,4,2048]{3,2,1,0:T(4,128)(2,1)S(1)} %get-tuple-element.7), channel_id=1, replica_groups=mesh['sp'=64,'tp'=4] {'sp'}, dimensions={0} | all-to-all | bytes 8388608 | tf_op jit(solution)/shard_map/all_to_all | solution.py:49
  254.4 7.2 %all-to-all-start.3 = ((bf16[64,4,4,2048]{3,2,1,0:T(4,128)(2,1)}), bf16[64,4,4,2048]{3,2,1,0:T(4,128)(2,1)}, u32[]{:S(2)}, u32[]{:S(2)}) async-start(bf16[64,4,4,2048]{3,2,1,0:T(4,128)(2,1)} %get-tuple-element.8), calls=%async_computation.4 | async-start | bytes 8388608 | tf_op jit(solution)/shard_map/all_to_all | solution.py:49
  261.6 6.9 %reshape.301 = bf16[1024,2048]{1,0:T(8,128)(2,1)} reshape(bf16[64,4,4,2048]{3,2,1,0:T(4,128)(2,1)} %all_to_all.26) | data formatting | bytes 8388608 | tf_op jit(solution)/shard_map/reshape | solution.py:118
  268.5 5.3 %fusion.11 = f32[1024,512]{1,0:T(8,128)S(1)} fusion(bf16[1024,2048]{1,0:T(8,128)(2,1)} %reshape.301, bf16[1,2048,512]{2,1,0:T(8,128)(2,1)} %param.22), kind=kOutput, calls=%fused_computation.22 | convolution fusion | flops 2147483648 | bytes 8388608 | tf_op jit(solution)/shard_map/dot_general | solution.py:120
  273.8 3.8 multiply_convert_fusion.1
  279.9 5.7 %convolution_convert_fusion.1 = bf16[64,4,4,2048]{3,0,2,1:T(8,128)(2,1)} fusion(bf16[1,512,2048]{2,1,0:T(8,128)(2,1)S(1)} %copy-done, bf16[64,4,4,512]{3,2,1,0:T(4,128)(2,1)} %dot_general.28), kind=kOutput, calls=%fused_computation.8 | convolution fusion | flops 2149580800 | bytes 7340032 | tf_op jit(solution)/shard_map/dot_general | solution.py:122
  285.9 70.5 %all-to-all-done.3 = bf16[64,4,4,2048]{3,2,1,0:T(4,128)(2,1)} async-done(((bf16[64,4,4,2048]{3,2,1,0:T(4,128)(2,1)}), bf16[64,4,4,2048]{3,2,1,0:T(4,128)(2,1)}, u32[]{:S(2)}, u32[]{:S(2)}) %all-to-all-start.3) | async-done | bytes 4194336 | tf_op jit(solution)/shard_map/all_to_all | solution.py:49
  356.4 6.9 %reshape.302 = bf16[1024,2048]{1,0:T(8,128)(2,1)} reshape(bf16[64,4,4,2048]{3,2,1,0:T(4,128)(2,1)} %all-to-all-done.3) | data formatting | bytes 8388608 | tf_op jit(solution)/shard_map/reshape | solution.py:118
  363.3 5.3 %fusion.9 = f32[1024,512]{1,0:T(8,128)S(1)} fusion(bf16[1024,2048]{1,0:T(8,128)(2,1)} %reshape.302, bf16[1,2048,512]{2,1,0:T(8,128)(2,1)} %param.22), kind=kOutput, calls=%fused_computation.20 | convolution fusion | flops 2147483648 | bytes 8388608 | tf_op jit(solution)/shard_map/dot_general | solution.py:120
  374.7 5.8 %convolution_convert_fusion = bf16[64,4,4,2048]{3,0,2,1:T(8,128)(2,1)} fusion(bf16[1,512,2048]{2,1,0:T(8,128)(2,1)S(1)} %copy-done, bf16[64,4,4,512]{3,2,1,0:T(4,128)(2,1)} %dot_general.32), kind=kOutput, calls=%fused_computation.7 | convolution fusion | flops 2149580800 | bytes 7340032 | tf_op jit(solution)/shard_map/dot_general | solution.py:122
  383.6 6.9 %all-to-all-start.2 = ((bf16[64,1,4,2048]{3,2,1,0:T(4,128)(2,1)}), bf16[64,1,4,2048]{3,2,1,0:T(4,128)(2,1)}, u32[]{:S(2)}, u32[]{:S(2)}) async-start(bf16[64,1,4,2048]{3,2,1,0:T(4,128)(2,1)} %copy.82), calls=%async_computation.3 | async-start | bytes 2097152 | tf_op jit(solution)/shard_map/all_to_all | solution.py:128
  390.5 35.8 %reduce-scatter.5.cloned.1.call-done = bf16[64,1,4,2048]{3,0,2,1:T(8,128)(2,1)} async-done(((bf16[64,4,4,2048]{3,0,2,1:T(8,128)(2,1)}), bf16[64,1,4,2048]{3,0,2,1:T(8,128)(2,1)}) %reduce-scatter.5.cloned.1.call-update) | async-done | bytes 1048592 | tf_op jit(solution)/shard_map/reduce_scatter | solution.py:125
  429.3 11.5 %all-to-all-start.4 = ((bf16[64,1,4,2048]{3,2,1,0:T(4,128)(2,1)}), bf16[64,1,4,2048]{3,2,1,0:T(4,128)(2,1)}, u32[]{:S(2)}, u32[]{:S(2)}) async-start(bf16[64,1,4,2048]{3,2,1,0:T(4,128)(2,1)} %copy.84), calls=%async_computation.6 | async-start | bytes 2097152 | tf_op jit(solution)/shard_map/all_to_all | solution.py:128
  442.9 25.8 %all-to-all-done.4 = bf16[64,1,4,2048]{3,2,1,0:T(4,128)(2,1)} async-done(((bf16[64,1,4,2048]{3,2,1,0:T(4,128)(2,1)}), bf16[64,1,4,2048]{3,2,1,0:T(4,128)(2,1)}, u32[]{:S(2)}, u32[]{:S(2)}) %all-to-all-start.4) | async-done | bytes 1048608 | tf_op jit(solution)/shard_map/all_to_all | solution.py:128
  468.7 4.0 maximum_bitcast_fusion
  472.7 6.9 %gather_fusion = bf16[384,2048]{1,0:T(8,128)(2,1)} fusion(bf16[512,2048]{1,0:T(8,128)(2,1)} %maximum_bitcast_fusion, s32[1024]{0:T(1024)S(1)} %pad_clamp_fusion.1), kind=kCustom, calls=%fused_computation.1 | custom fusion | bytes 3147264 | tf_op jit(solution)/shard_map/gather | solution.py:134
  483.3 4.4 fusion.48
  (84 shorter events, 38.0 us)
Async XLA Ops:
  6.5 273.3 %copy-start = (bf16[1,512,2048]{2,1,0:T(8,128)(2,1)S(1)}, bf16[1,512,2048]{2,1,0:T(8,128)(2,1)}, u32[]{:S(2)}) copy-start(bf16[1,512,2048]{2,1,0:T(8,128)(2,1)} %param.23) | copy-start | bytes 6291460
  6.5 10.9 %copy-start.5 = (bf16[768,256]{1,0:T(8,128)(2,1)S(1)}, bf16[768,256]{1,0:T(8,128)(2,1)}, u32[]{:S(2)}) copy-start(bf16[768,256]{1,0:T(8,128)(2,1)} %param.14) | copy-start | bytes 1179652
  6.5 10.9 %copy-start.3 = (bf16[256,2048]{1,0:T(8,128)(2,1)S(1)}, bf16[256,2048]{1,0:T(8,128)(2,1)}, u32[]{:S(2)}) copy-start(bf16[256,2048]{1,0:T(8,128)(2,1)} %param.16) | copy-start | bytes 3145732
  6.5 99.5 %all-gather.3.cloned.1.call-start = ((), (), s32[]{:S(2)}) async-start(), calls=%async_computation.7 | async-start | bytes 3932160 | tf_op jit(solution)/shard_map/all_gather | solution.py:100
  7.9 7.2 %collective-permute-start = (bf16[1,256]{1,0:T(2,128)(2,1)S(1)}, bf16[1,256]{1,0:T(2,128)(2,1)S(1)}, u32[]{:S(2)}, u32[]{:S(2)}) collective-permute-start(bf16[1,256]{1,0:T(2,128)(2,1)S(1)} %get-tuple-element.11), channel_id=1, source_target_pairs={{0,4},{4,8},{8,12},{12,16},{16,20},{20,24},{24,28},{28,32},{32,36}... | collective-permute-start | bytes 1544 | tf_op jit(solution)/shard_map/ppermute | solution.py:18
  12.4 4.9 collective-permute-start.1
  59.3 1.1 copy-start.4
  60.4 0.7 copy-start.7
  60.4 1.8 copy-start.6
  254.4 102.0 %all-to-all-start.3 = ((bf16[64,4,4,2048]{3,2,1,0:T(4,128)(2,1)}), bf16[64,4,4,2048]{3,2,1,0:T(4,128)(2,1)}, u32[]{:S(2)}, u32[]{:S(2)}) async-start(bf16[64,4,4,2048]{3,2,1,0:T(4,128)(2,1)} %get-tuple-element.8), calls=%async_computation.4 | async-start | bytes 8388608 | tf_op jit(solution)/shard_map/all_to_all | solution.py:49
  261.5 119.0 %reduce-scatter.3.cloned.1.call-start = ((), (), s32[]{:S(2)}) async-start(), calls=%async_computation.8 | async-start | bytes 5242880 | tf_op jit(solution)/shard_map/reduce_scatter | solution.py:125
  268.5 5.3 %copy-start.1 = (bf16[1024,2048]{1,0:T(8,128)(2,1)S(1)}, bf16[1024,2048]{1,0:T(8,128)(2,1)}, u32[]{:S(2)}) copy-start(bf16[1024,2048]{1,0:T(8,128)(2,1)} %reshape.301) | copy-start | bytes 12582916
  268.5 5.3 %copy-start.9 = (bf16[1,2048,512]{2,1,0:T(8,128)(2,1)S(1)}, bf16[1,2048,512]{2,1,0:T(8,128)(2,1)}, u32[]{:S(2)}) copy-start(bf16[1,2048,512]{2,1,0:T(8,128)(2,1)} %param.21) | copy-start | bytes 6291460
  285.6 140.7 %reduce-scatter.5.cloned.1.call-start = ((), (), s32[]{:S(2)}) async-start(), calls=%async_computation.9 | async-start | bytes 5242880 | tf_op jit(solution)/shard_map/reduce_scatter | solution.py:125
  363.3 5.3 %copy-start.2 = (bf16[1024,2048]{1,0:T(8,128)(2,1)S(1)}, bf16[1024,2048]{1,0:T(8,128)(2,1)}, u32[]{:S(2)}) copy-start(bf16[1024,2048]{1,0:T(8,128)(2,1)} %reshape.302) | copy-start | bytes 12582916
  363.3 5.3 %copy-start.10 = (bf16[1,2048,512]{2,1,0:T(8,128)(2,1)S(1)}, bf16[1,2048,512]{2,1,0:T(8,128)(2,1)}, u32[]{:S(2)}) copy-start(bf16[1,2048,512]{2,1,0:T(8,128)(2,1)} %param.21) | copy-start | bytes 6291460
  383.6 45.8 %all-to-all-start.2 = ((bf16[64,1,4,2048]{3,2,1,0:T(4,128)(2,1)}), bf16[64,1,4,2048]{3,2,1,0:T(4,128)(2,1)}, u32[]{:S(2)}, u32[]{:S(2)}) async-start(bf16[64,1,4,2048]{3,2,1,0:T(4,128)(2,1)} %copy.82), calls=%async_computation.3 | async-start | bytes 2097152 | tf_op jit(solution)/shard_map/all_to_all | solution.py:128
  429.3 13.6 %copy-start.8 = (f32[192,2]{0,1:T(2,128)S(1)}, f32[192,2]{0,1:T(2,128)}, u32[]{:S(2)}) copy-start(f32[192,2]{0,1:T(2,128)} %param.20) | copy-start | bytes 4612
  429.3 39.4 %all-to-all-start.4 = ((bf16[64,1,4,2048]{3,2,1,0:T(4,128)(2,1)}), bf16[64,1,4,2048]{3,2,1,0:T(4,128)(2,1)}, u32[]{:S(2)}, u32[]{:S(2)}) async-start(bf16[64,1,4,2048]{3,2,1,0:T(4,128)(2,1)} %copy.84), calls=%async_computation.6 | async-start | bytes 2097152 | tf_op jit(solution)/shard_map/all_to_all | solution.py:128
Sparse Core Ops, SparseCore 0:
  62.4 43.6 all-gather.2
  285.8 49.2 reduce-scatter.2
  380.6 45.6 reduce-scatter.4
where the time goes:
time: 503 us; the launch traced here: 497 us
  waiting for transfers between devices  159 us (32%)
  blocking collectives  154 us (31%)
  local copies, waits for them, and re-layouts  88 us (17%)
  starting transfers between devices  32.3 us (6%)
  matrix products  30.9 us (6%)
  other arithmetic  19.3 us (4%)
  between operations  13.7 us (3%)
    all_to_all x1, blocking collectives, grouped_exchange(): lax.all_to_all(group, axis, split_axis=split_dim, concat_axis=concat_dim,...  105 us
    all_to_all x1, waiting for transfers between devices, grouped_exchange(): lax.all_to_all(group, axis, split_axis=split_dim, concat_axis=concat_dim,...  70.5 us
    all_to_all x1, blocking collectives, sent_and_summed(): lax.all_to_all(pieces, axis, split_axis=0, concat_axis=0, tiled=True)  40.7 us
    reduce_scatter x2, waiting for transfers between devices, expert_work(): lax.psum_scatter(partial_value.astype(jnp.bfloat16), 'tp', scatter_dimens...  35.8 us
    scatter x1, local copies, waits for them, and re-layouts, local(): outgoing = outgoing.at[targets].set(group_rows[entry_ids // top_count])  31.9 us
    all_to_all x2, waiting for transfers between devices, expert_work(): return lax.all_to_all(summed, 'sp', split_axis=0, concat_axis=0, tiled=True)  25.8 us
    all_gather x1, waiting for transfers between devices, local(): lax.all_gather(normed, 'tp', axis=0, tiled=True)  24.4 us
    all_to_all x2, starting transfers between devices, expert_work(): return lax.all_to_all(summed, 'sp', split_axis=0, concat_axis=0, tiled=True)  18.4 us
  transfers between devices with their start and end apart: 8, of which 5 were waited for; matrix products, arithmetic and copies ran while one was open for 14% of the time, Pallas kernels for 0%

commit v1 on v0

v1 whole, which is shorter than its diff:
```python
import jax
import jax.numpy as jnp
from jax import lax
from jax.sharding import PartitionSpec as P

EPSILON = 1e-05
LIMIT = 7.0
ALPHA = 1.702
CAP = 8


def with_halo(x, axis):
    count, length = lax.axis_size(axis), x.shape[0]
    up = [(i, (i + 1) % count) for i in range(count - 1)]
    down = [(j, i) for i, j in up]
    before = lax.ppermute(x[length - 1 :], axis, up)
    after = lax.ppermute(x[:1], axis, down)
    return jnp.concatenate([before, x, after], axis=0)


def clamped_unit(gate_pre, up_pre):
    gated = jnp.minimum(gate_pre, LIMIT)
    upward = jnp.clip(up_pre, -LIMIT, LIMIT)
    return (upward + 1.0) * gated * jax.nn.sigmoid(ALPHA * gated)


def local(
    conv_in,
    conv_pre,
    conv_post,
    taps,
    out_proj,
    stream,
    norm_gain,
    routes,
    route_weight,
    gate_w,
    up_w,
    down_w,
):
    product = conv_pre.astype(jnp.float32) * conv_in.astype(jnp.float32)
    padded = with_halo(product.astype(jnp.bfloat16), "sp").astype(product.dtype)
    convolved = taps[0] * padded[:-2] + taps[1] * padded[1:-1] + taps[2] * padded[2:]
    mixed = (conv_post.astype(jnp.float32) * convolved).astype(jnp.bfloat16)
    own_rows, width = stream.shape
    part = jnp.dot(mixed, out_proj, preferred_element_type=jnp.float32).astype(jnp.bfloat16)
    part = part.reshape(lax.axis_size("tp"), own_rows, width)
    branch = lax.all_to_all(part, "tp", split_axis=0, concat_axis=0, tiled=True)
    branch = branch.astype(jnp.float32).sum(axis=0)
    resid = (stream.astype(jnp.float32) + branch).astype(jnp.bfloat16)
    resid_f = resid.astype(jnp.float32)
    scale = lax.rsqrt(jnp.mean(resid_f * resid_f, axis=-1, keepdims=True) + EPSILON)
    normed = (resid_f * scale * norm_gain).astype(jnp.bfloat16)

    experts = lax.axis_size("sp")
    top = routes.shape[1]
    flat = routes.reshape(-1)
    onehot = (flat[:, None] == jnp.arange(experts, dtype=jnp.int32)[None, :]).astype(jnp.bfloat16)
    entry = jnp.arange(own_rows * top, dtype=jnp.int32)
    earlier = (entry[None, :] < entry[:, None]).astype(jnp.bfloat16)
    counts = jnp.dot(earlier, onehot, preferred_element_type=jnp.float32)
    rank = jnp.sum(counts * onehot.astype(jnp.float32), axis=1).astype(jnp.int32)
    slots = experts * CAP
    target = (flat * CAP + rank).reshape(own_rows, top)
    ids = jnp.arange(slots, dtype=jnp.int32)[None, None, :]
    chosen = target[:, :, None] == ids
    pick = chosen.any(axis=1).astype(jnp.bfloat16)
    outgoing = lax.dot_general(
        pick, normed, (((0,), (0,)), ((), ())), preferred_element_type=jnp.float32
    ).astype(jnp.bfloat16)
    outgoing = outgoing.reshape(experts, CAP, width)
    done = []
    for k in range(2):
        group = outgoing[:, k * 4 : (k + 1) * 4]
        arrived = lax.all_to_all(group, "sp", split_axis=0, concat_axis=0, tiled=True)
        rows = lax.all_gather(arrived.reshape(-1, width), "tp", axis=0, tiled=True)
        gate_pre = jnp.dot(rows, gate_w[0], preferred_element_type=jnp.float32)
        up_pre = jnp.dot(rows, up_w[0], preferred_element_type=jnp.float32)
        active = clamped_unit(gate_pre, up_pre).astype(jnp.bfloat16)
        partial = jnp.dot(active, down_w[0], preferred_element_type=jnp.float32)
        summed = lax.psum_scatter(
            partial.astype(jnp.bfloat16), "tp", scatter_dimension=0, tiled=True
        )
        done.append(
            lax.all_to_all(
                summed.reshape(experts, 4, width), "sp", split_axis=0, concat_axis=0, tiled=True
            )
        )
    spread = jnp.sum(jnp.where(chosen, route_weight[:, :, None], 0.0), axis=1)
    total = resid.astype(jnp.float32)
    for k in range(2):
        share = spread.reshape(own_rows, experts, CAP)[:, :, k * 4 : (k + 1) * 4]
        share = share.reshape(own_rows, -1)
        high = share.astype(jnp.bfloat16)
        low = (share - high.astype(jnp.float32)).astype(jnp.bfloat16)
        back = done[k].reshape(-1, width)
        total = total + jnp.dot(high, back, preferred_element_type=jnp.float32)
        total = total + jnp.dot(low, back, preferred_element_type=jnp.float32)
    return total.astype(jnp.bfloat16)


def solution(mesh):
    placed = (
        P("sp", "tp"),
        P("sp", "tp"),
        P("sp", "tp"),
        P(None, "tp"),
        P("tp", None),
        P(("sp", "tp"), None),
        P(),
        P(("sp", "tp"), None),
        P(("sp", "tp"), None),
        P("sp", None, "tp"),
        P("sp", None, "tp"),
        P("sp", "tp", None),
    )
    return jax.shard_map(
        local, mesh=mesh, in_specs=placed, out_specs=P(("sp", "tp"), None), check_vma=False
    )
```

time: 503 us -> 368 us (0.73); the launches traced: 497 us -> 367 us
  blocking collectives: 154 us -> 75 us
  local copies, waits for them, and re-layouts: 88 us -> 14.8 us
  matrix products: 30.9 us -> 49.1 us
  waiting for transfers between devices: 159 us -> 177 us
  other arithmetic: 19.3 us -> 4.81 us
    all_to_all x2, blocking collectives: 146 us -> 75 us  [local(): lax.all_to_all(group, 'sp', split_axis=0, concat_axis=0, tiled=True)]
    all_to_all x3, waiting for transfers between devices: 96.3 us -> 54.8 us  [the longest x1 35.6 us: local(): branch = lax.all_to_all(part, 'tp', split_axis=0, concat_axis=0, tiled=True)]
    reduce_scatter x2, waiting for transfers between devices: 35.8 us -> 74.2 us  [local(): lax.psum_scatter(partial.astype(jnp.bfloat16), 'tp', scatter_dimension=0,...]
    scatter x1 -> x0, local copies, waits for them, and re-layouts: 31.9 us -> none  [local(): outgoing = outgoing.at[targets].set(group_rows[entry_ids // top_count])]
    all_gather x1 -> x2, waiting for transfers between devices: 24.4 us -> 46 us  [local(): rows = lax.all_gather(arrived.reshape(-1, width), 'tp', axis=0, tiled=True)]
    dot_general x6 -> x10, matrix products: 29.8 us -> 46.3 us  [the longest x2 20.6 us: local(): partial = jnp.dot(active, down_w[0], preferred_element_type=jnp.float32)]
    slice x6 -> x3, local copies, waits for them, and re-layouts: 17.6 us -> 3.53 us  [the longest x1 2.14 us: local(): group = outgoing[:, k * 4:(k + 1) * 4]]
    reshape x3 -> x4, local copies, waits for them, and re-layouts: 17.6 us -> 6.77 us  [the longest x2 4.48 us: local(): summed.reshape(experts, 4, width)]
  transfers between devices with their start and end apart: 8 -> 9, of which waited for: 5 -> 7; matrix products, arithmetic and copies ran while one was open for 14% -> 14% of each run, Pallas kernels for 0% -> 0%
where the time goes in v1:
time: 368 us; the launch traced here: 367 us
  waiting for transfers between devices  177 us (48%)
  blocking collectives  75 us (20%)
  matrix products  49.1 us (13%)
  starting transfers between devices  33 us (9%)
  local copies, waits for them, and re-layouts  14.8 us (4%)
  between operations  13.4 us (4%)
  other arithmetic  4.81 us (1%)
    all_to_all x2, blocking collectives, local(): lax.all_to_all(group, 'sp', split_axis=0, concat_axis=0, tiled=True)  75 us
    reduce_scatter x2, waiting for transfers between devices, local(): lax.psum_scatter(partial.astype(jnp.bfloat16), 'tp', scatter_dimension=0,...  74.2 us
    all_gather x2, waiting for transfers between devices, local(): rows = lax.all_gather(arrived.reshape(-1, width), 'tp', axis=0, tiled=True)  46 us
    all_to_all x1, waiting for transfers between devices, local(): branch = lax.all_to_all(part, 'tp', split_axis=0, concat_axis=0, tiled=True)  35.6 us
    all_to_all x2, starting transfers between devices, local(): lax.all_to_all(summed.reshape(experts, 4, width), 'sp', split_axis=0, con...  21.4 us
    dot_general x2, matrix products, local(): partial = jnp.dot(active, down_w[0], preferred_element_type=jnp.float32)  20.6 us
    all_to_all x2, waiting for transfers between devices, local(): lax.all_to_all(summed.reshape(experts, 4, width), 'sp', split_axis=0, con...  19.3 us
    dot_general x2, matrix products, local(): up_pre = jnp.dot(rows, up_w[0], preferred_element_type=jnp.float32)  13.1 us
  transfers between devices with their start and end apart: 9, of which 7 were waited for; matrix products, arithmetic and copies ran while one was open for 14% of the time, Pallas kernels for 0%

profile of v1, /device:TPU:1, one launch (start us, length us, event | category | flops | bytes accessed | tf_op | source)
XLA Modules:
  0.0 367.3 jit_solution(12065180576500988461)
XLA Ops:
  7.9 4.5 %collective-permute-start = (bf16[1,256]{1,0:T(2,128)(2,1)S(1)}, bf16[1,256]{1,0:T(2,128)(2,1)S(1)}, u32[]{:S(2)}, u32[]{:S(2)}) collective-permute-start(bf16[1,256]{1,0:T(2,128)(2,1)S(1)} %get-tuple-element.11), channel_id=1, source_target_pairs={{0,4},{4,8},{8,12},{12,16},{16,20},{20,24},{24,28},{28,32},{32,36}... | collective-permute-start | bytes 1544 | tf_op jit(solution)/shard_map/ppermute | solution.py:16
  15.2 2.2 collective-permute-done.1
  17.4 2.8 convolution_convert_fusion.2
  20.2 4.8 %all-to-all-start = ((bf16[4,192,2048]{2,1,0:T(8,128)(2,1)}), bf16[4,192,2048]{2,1,0:T(8,128)(2,1)}, u32[]{:S(2)}, u32[]{:S(2)}) async-start(bf16[4,192,2048]{2,1,0:T(8,128)(2,1)} %bitcast.54), calls=%async_computation | async-start | bytes 6291456 | tf_op jit(solution)/shard_map/all_to_all | solution.py:48
  26.0 35.6 %all-to-all-done = bf16[4,192,2048]{2,1,0:T(8,128)(2,1)} async-done(((bf16[4,192,2048]{2,1,0:T(8,128)(2,1)}), bf16[4,192,2048]{2,1,0:T(8,128)(2,1)}, u32[]{:S(2)}, u32[]{:S(2)}) %all-to-all-start) | async-done | bytes 3145760 | tf_op jit(solution)/shard_map/all_to_all | solution.py:48
  61.6 2.7 convert_reduce_fusion
  68.5 40.6 %all_to_all.25 = bf16[64,4,2048]{2,1,0:T(4,128)(2,1)S(1)} all-to-all(bf16[64,4,2048]{2,1,0:T(4,128)(2,1)S(1)} %get-tuple-element.8), channel_id=1, replica_groups=mesh['sp'=64,'tp'=4] {'sp'}, dimensions={0} | all-to-all | bytes 2097152 | tf_op jit(solution)/shard_map/all_to_all | solution.py:75
  110.3 34.4 %all_to_all.26 = bf16[64,4,2048]{2,1,0:T(4,128)(2,1)S(1)} all-to-all(bf16[64,4,2048]{2,1,0:T(4,128)(2,1)} %get-tuple-element.7), channel_id=1, replica_groups=mesh['sp'=64,'tp'=4] {'sp'}, dimensions={0} | all-to-all | bytes 2097152 | tf_op jit(solution)/shard_map/all_to_all | solution.py:75
  146.1 9.9 %all-gather.5.cloned.1.call-done = bf16[1024,2048]{1,0:T(8,128)(2,1)} async-done(((bf16[256,2048]{1,0:T(8,128)(2,1)}), bf16[1024,2048]{1,0:T(8,128)(2,1)}) %all-gather.5.cloned.1.call-update) | async-done | bytes 4194320 | tf_op jit(solution)/shard_map/all_gather | solution.py:76
  156.1 6.6 %fusion.12 = f32[1024,512]{1,0:T(8,128)} fusion(bf16[1024,2048]{1,0:T(8,128)(2,1)} %all-gather.5.cloned.1.call-done, bf16[1,2048,512]{2,1,0:T(8,128)(2,1)} %param.22), kind=kOutput, calls=%fused_computation.23 | convolution fusion | flops 2147483648 | bytes 8388608 | tf_op jit(solution)/shard_map/dot_general | solution.py:78
  162.7 10.3 %convolution_convert_fusion = bf16[1024,2048]{1,0:T(8,128)(2,1)} fusion(bf16[1,512,2048]{2,1,0:T(8,128)(2,1)S(1)} %copy-done, f32[1024,512]{1,0:T(8,128)} %fusion.12, bf16[1024,2048]{1,0:T(8,128)(2,1)} %all-gather.5.cloned.1.call-done, bf16[1,2048,512]{2,1,0:T(8,128)(2,1)} %param.21), kind=kOutput, calls=%fused_computation.1 | convolution fusion | flops 4302307328 | bytes 14680064 | tf_op jit(solution)/shard_map/dot_general | solution.py:80
  173.0 36.0 %all-gather.3.cloned.1.call-done = bf16[1024,2048]{1,0:T(8,128)(2,1)} async-done(((bf16[256,2048]{1,0:T(8,128)(2,1)}), bf16[1024,2048]{1,0:T(8,128)(2,1)}) %all-gather.3.cloned.1.call-update) | async-done | bytes 4194320 | tf_op jit(solution)/shard_map/all_gather | solution.py:76
  209.1 6.5 %fusion.14 = f32[1024,512]{1,0:T(8,128)} fusion(bf16[1024,2048]{1,0:T(8,128)(2,1)} %all-gather.3.cloned.1.call-done, bf16[1,2048,512]{2,1,0:T(8,128)(2,1)} %param.22), kind=kOutput, calls=%fused_computation.25 | convolution fusion | flops 2147483648 | bytes 8388608 | tf_op jit(solution)/shard_map/dot_general | solution.py:78
  215.6 10.3 %convolution_convert_fusion.1 = bf16[1024,2048]{1,0:T(8,128)(2,1)} fusion(bf16[1,512,2048]{2,1,0:T(8,128)(2,1)S(1)} %copy-done, f32[1024,512]{1,0:T(8,128)} %fusion.14, bf16[1024,2048]{1,0:T(8,128)(2,1)} %all-gather.3.cloned.1.call-done, bf16[1,2048,512]{2,1,0:T(8,128)(2,1)} %param.21), kind=kOutput, calls=%fused_computation.2 | convolution fusion | flops 4302307328 | bytes 14680064 | tf_op jit(solution)/shard_map/dot_general | solution.py:80
  225.9 35.6 %reduce-scatter.5.cloned.1.call-done = bf16[256,2048]{1,0:T(8,128)(2,1)} async-done(((bf16[1024,2048]{1,0:T(8,128)(2,1)}), bf16[256,2048]{1,0:T(8,128)(2,1)}) %reduce-scatter.5.cloned.1.call-update) | async-done | bytes 1048592 | tf_op jit(solution)/shard_map/reduce_scatter | solution.py:81
  261.5 2.2 reshape.56
  263.7 10.7 %all-to-all-start.4 = ((bf16[64,4,2048]{2,1,0:T(4,128)(2,1)}), bf16[64,4,2048]{2,1,0:T(4,128)(2,1)S(1)}, u32[]{:S(2)}, u32[]{:S(2)}) async-start(bf16[64,4,2048]{2,1,0:T(4,128)(2,1)} %reshape.56), calls=%async_computation.6 | async-start | bytes 2097152 | tf_op jit(solution)/shard_map/all_to_all | solution.py:85
  274.5 38.6 %reduce-scatter.3.cloned.1.call-done = bf16[256,2048]{1,0:T(8,128)(2,1)} async-done(((bf16[1024,2048]{1,0:T(8,128)(2,1)}), bf16[256,2048]{1,0:T(8,128)(2,1)}) %reduce-scatter.3.cloned.1.call-update) | async-done | bytes 1048592 | tf_op jit(solution)/shard_map/reduce_scatter | solution.py:81
  313.1 2.3 reshape.54
  316.4 10.7 %all-to-all-start.2 = ((bf16[64,4,2048]{2,1,0:T(4,128)(2,1)}), bf16[64,4,2048]{2,1,0:T(4,128)(2,1)S(1)}, u32[]{:S(2)}, u32[]{:S(2)}) async-start(bf16[64,4,2048]{2,1,0:T(4,128)(2,1)} %reshape.54), calls=%async_computation.3 | async-start | bytes 2097152 | tf_op jit(solution)/shard_map/all_to_all | solution.py:85
  329.7 3.8 %convolution_bitcast_fusion.1 = f32[192,2048]{1,0:T(8,128)} fusion(bf16[64,4,2048]{2,1,0:T(4,128)(2,1)} %copy-done.1, f32[192,64,4]{0,2,1:T(4,128)S(1)} %get-tuple-element.10), kind=kOutput, calls=%fused_computation.7 | convolution fusion | flops 201326592 | bytes 2818048 | tf_op jit(solution)/shard_map/dot_general | solution.py:97
  333.5 2.5 convolution_bitcast_fusion
  336.0 19.3 %all-to-all-done.2 = bf16[64,4,2048]{2,1,0:T(4,128)(2,1)S(1)} async-done(((bf16[64,4,2048]{2,1,0:T(4,128)(2,1)}), bf16[64,4,2048]{2,1,0:T(4,128)(2,1)S(1)}, u32[]{:S(2)}, u32[]{:S(2)}) %all-to-all-start.2) | async-done | bytes 1048608 | tf_op jit(solution)/shard_map/all_to_all | solution.py:85
  356.9 3.9 %fusion.5 = bf16[192,2048]{1,0:T(8,128)(2,1)} fusion(f32[192,2048]{1,0:T(8,128)} %convolution_bitcast_fusion, f32[192,2048]{1,0:T(8,128)S(1)} %copy-done.5, f32[192,2048]{1,0:T(8,128)S(1)} %convolution_bitcast_fusion.2, bf16[192,2048]{1,0:T(8,128)(2,1)S(1)} %copy-done.4, bf16[64,4,2048]{2,1,0:T(4,128)(2,1)S(1)} %all-to-all-done.2, ...), kind=kOutput, calls=%fused_computation.14 | convolution fusion | flops 203685888 | bytes 7536640 | tf_op jit(solution)/shard_map/dot_general | solution.py:97
  (57 shorter events, 17.1 us)
Async XLA Ops:
  6.5 156.1 %copy-start = (bf16[1,512,2048]{2,1,0:T(8,128)(2,1)S(1)}, bf16[1,512,2048]{2,1,0:T(8,128)(2,1)}, u32[]{:S(2)}) copy-start(bf16[1,512,2048]{2,1,0:T(8,128)(2,1)} %param.23) | copy-start | bytes 6291460
  6.5 10.9 %copy-start.8 = (bf16[768,256]{1,0:T(8,128)(2,1)S(1)}, bf16[768,256]{1,0:T(8,128)(2,1)}, u32[]{:S(2)}) copy-start(bf16[768,256]{1,0:T(8,128)(2,1)} %param.14) | copy-start | bytes 1179652
  6.5 10.9 %copy-start.6 = (bf16[256,2048]{1,0:T(8,128)(2,1)S(1)}, bf16[256,2048]{1,0:T(8,128)(2,1)}, u32[]{:S(2)}) copy-start(bf16[256,2048]{1,0:T(8,128)(2,1)} %param.16) | copy-start | bytes 3145732
  7.9 7.2 %collective-permute-start = (bf16[1,256]{1,0:T(2,128)(2,1)S(1)}, bf16[1,256]{1,0:T(2,128)(2,1)S(1)}, u32[]{:S(2)}, u32[]{:S(2)}) collective-permute-start(bf16[1,256]{1,0:T(2,128)(2,1)S(1)} %get-tuple-element.11), channel_id=1, source_target_pairs={{0,4},{4,8},{8,12},{12,16},{16,20},{20,24},{24,28},{28,32},{32,36}... | collective-permute-start | bytes 1544 | tf_op jit(solution)/shard_map/ppermute | solution.py:16
  12.4 4.9 %collective-permute-start.1 = (bf16[1,256]{1,0:T(2,128)(2,1)S(1)}, bf16[1,256]{1,0:T(2,128)(2,1)S(1)}, u32[]{:S(2)}, u32[]{:S(2)}) collective-permute-start(bf16[1,256]{1,0:T(2,128)(2,1)S(1)} %get-tuple-element.12), channel_id=1, source_target_pairs={{4,0},{8,4},{12,8},{16,12},{20,16},{24,20},{28,24},{32,28},{36,32}... | collective-permute-start | bytes 1544 | tf_op jit(solution)/shard_map/ppermute | solution.py:17
  20.2 4.9 %copy-start.10 = (s32[192,2]{0,1:T(2,128)S(1)}, s32[192,2]{0,1:T(2,128)}, u32[]{:S(2)}) copy-start(s32[192,2]{0,1:T(2,128)} %param.19) | copy-start | bytes 4612
  20.2 41.3 %all-to-all-start = ((bf16[4,192,2048]{2,1,0:T(8,128)(2,1)}), bf16[4,192,2048]{2,1,0:T(8,128)(2,1)}, u32[]{:S(2)}, u32[]{:S(2)}) async-start(bf16[4,192,2048]{2,1,0:T(8,128)(2,1)} %bitcast.54), calls=%async_computation | async-start | bytes 6291456 | tf_op jit(solution)/shard_map/all_to_all | solution.py:48
  25.0 131.0 %all-gather.5.cloned.1.call-start = ((), (), s32[]{:S(2)}) async-start(), calls=%async_computation.9 | async-start | bytes 5242880 | tf_op jit(solution)/shard_map/all_gather | solution.py:76
  26.0 38.3 %copy-start.7 = (bf16[192,2048]{1,0:T(8,128)(2,1)S(1)}, bf16[192,2048]{1,0:T(8,128)(2,1)}, u32[]{:S(2)}) copy-start(bf16[192,2048]{1,0:T(8,128)(2,1)} %param.17) | copy-start | bytes 2359300
  64.3 1.2 copy-start.9
  64.6 0.9 copy-start.3
  110.3 98.8 %all-gather.3.cloned.1.call-start = ((), (), s32[]{:S(2)}) async-start(), calls=%async_computation.7 | async-start | bytes 5242880 | tf_op jit(solution)/shard_map/all_gather | solution.py:76
  145.9 115.6 %reduce-scatter.5.cloned.1.call-start = ((), (), s32[]{:S(2)}) async-start(), calls=%async_computation.10 | async-start | bytes 5242880 | tf_op jit(solution)/shard_map/reduce_scatter | solution.py:81
  173.0 140.1 %reduce-scatter.3.cloned.1.call-start = ((), (), s32[]{:S(2)}) async-start(), calls=%async_computation.8 | async-start | bytes 5242880 | tf_op jit(solution)/shard_map/reduce_scatter | solution.py:81
  263.7 51.6 %all-to-all-start.4 = ((bf16[64,4,2048]{2,1,0:T(4,128)(2,1)}), bf16[64,4,2048]{2,1,0:T(4,128)(2,1)S(1)}, u32[]{:S(2)}, u32[]{:S(2)}) async-start(bf16[64,4,2048]{2,1,0:T(4,128)(2,1)} %reshape.56), calls=%async_computation.6 | async-start | bytes 2097152 | tf_op jit(solution)/shard_map/all_to_all | solution.py:85
  274.5 52.6 %copy-start.11 = (f32[192,2]{0,1:T(2,128)S(1)}, f32[192,2]{0,1:T(2,128)}, u32[]{:S(2)}) copy-start(f32[192,2]{0,1:T(2,128)} %param.20) | copy-start | bytes 4612
  315.4 1.0 copy-start.1
  316.4 38.9 %all-to-all-start.2 = ((bf16[64,4,2048]{2,1,0:T(4,128)(2,1)}), bf16[64,4,2048]{2,1,0:T(4,128)(2,1)S(1)}, u32[]{:S(2)}, u32[]{:S(2)}) async-start(bf16[64,4,2048]{2,1,0:T(4,128)(2,1)} %reshape.54), calls=%async_computation.3 | async-start | bytes 2097152 | tf_op jit(solution)/shard_map/all_to_all | solution.py:85
  328.3 5.2 %copy-start.2 = (bf16[64,4,2048]{2,1,0:T(4,128)(2,1)S(1)}, bf16[64,4,2048]{2,1,0:T(4,128)(2,1)}, u32[]{:S(2)}) copy-start(bf16[64,4,2048]{2,1,0:T(4,128)(2,1)} %copy-done.1) | copy-start | bytes 3145732
  355.3 1.4 copy-start.4
  355.3 1.7 copy-start.5
Sparse Core Ops, SparseCore 0:
  110.4 45.6 all-gather.4
  157.9 51.1 all-gather.2
  211.6 49.8 reduce-scatter.4
  263.9 49.1 reduce-scatter.2
